TPU v7x, 32 devices: a whole 2x2x4 slice. The times are simulated.
32 devices in a mesh: kv: 8 (over z, x), tp: 4 (over y, core).
Axes of the slice: x: 2, y: 2, z: 4, core: 2. Of those that a mesh axis runs over, the one named last changes fastest.
Arguments:
- hidden_in: bfloat16 [24, 4096], P('kv'), may hold values from -6 to 6
- norm_gain: float32 [4096], replicated, may hold values from 0.1 to 1.9
- w_query: bfloat16 [4096, 2048], P('kv', 'tp'), may hold values from -0.09375 to 0.09375
- w_key: bfloat16 [4096, 2048], P('kv', 'tp'), may hold values from -0.09375 to 0.09375
- w_value: bfloat16 [4096, 4096], P('kv', 'tp'), may hold values from -0.09375 to 0.09375
- w_out: bfloat16 [4096, 4096], P('kv', 'tp'), may hold values from -0.09375 to 0.09375
- carried_state: float32 [8, 8, 256, 512], P('kv', 'tp'), may hold values from -0.625 to 0.625
- prior_keys: bfloat16 [8, 8, 3, 256], P('kv', 'tp'), may hold values from -0.375 to 0.375
- prior_values: bfloat16 [8, 8, 3, 512], P('kv', 'tp'), may hold values from -6 to 6
- accepted: int32 [8], P('kv'), may hold values from 0 to 3
- lengths: int32 [8], P('kv'), may hold values from 1 to 4096
Outputs:
- layer_out: bfloat16 [24, 4096], P('tp', 'kv')
- committed_state: float32 [8, 8, 256, 512], P('kv', 'tp')
- new_keys: bfloat16 [8, 8, 3, 256], P('kv', 'tp')
- new_values: bfloat16 [8, 8, 3, 512], P('kv', 'tp')
All inputs are finite; a program needn't handle non-finite values.
Results may differ from a plain program's by a relative error of at most 0.014.
Values may be sent and summed in bfloat16 or wider, within the bound.
A program may use at most 64 MiB of HBM per device.

v0:
```python
import jax
import jax.numpy as jnp
from jax import lax
from jax.sharding import PartitionSpec as P

epsilon = 1e-06
rotary_base = 10000.0


def rotate(values, places):
    middle = values.shape[-1] // 2
    inverse = rotary_base ** (-jnp.linspace(0.0, 1.0, middle, dtype=jnp.float32))
    angles = places[..., None] * inverse
    cosine = jnp.cos(angles)[:, :, None, :]
    sine_term = jnp.sin(angles)[:, :, None, :]
    leading = values[..., :middle]
    trailing = values[..., middle:]
    return jnp.concatenate(
        [leading * cosine - trailing * sine_term, leading * sine_term + trailing * cosine], axis=-1
    )


def retain(
    queries,
    key_rows,
    value_rows,
    carried_state,
    prior_keys,
    prior_values,
    accepted,
    lengths,
    head_ids,
):
    steps_ahead = queries.shape[1]
    key_size = queries.shape[-1]
    log_decay = jnp.log(1.0 - 2.0 ** (-5.0 - head_ids))
    slot_ids = jnp.arange(steps_ahead, dtype=jnp.float32)
    places = (lengths + accepted).astype(jnp.float32)[:, None] + slot_ids[None, :]
    turned_q = rotate(queries.astype(jnp.float32), places)
    turned_k = rotate(key_rows.astype(jnp.float32), places) * key_size ** (-0.5)
    taken_count = accepted.astype(jnp.float32)[:, None]
    lag_steps = taken_count[:, :, None] - 1.0 - slot_ids[None, None, :]
    weights_back = jnp.where(
        lag_steps >= 0.0, jnp.exp(log_decay[None, :, None] * jnp.maximum(lag_steps, 0.0)), 0.0
    )
    keep_factor = jnp.exp(log_decay[None, :] * taken_count)
    scaled_keys = prior_keys.astype(jnp.float32) * weights_back[..., None]
    committed = keep_factor[..., None, None] * carried_state + jnp.einsum(
        "shjd,shje->shde",
        scaled_keys,
        prior_values.astype(jnp.float32),
        precision=lax.Precision.HIGHEST,
    )
    reach_decay = jnp.exp(log_decay[None, :] * (slot_ids[:, None] + 1.0))
    carried_part = (
        jnp.einsum("sihd,shde->sihe", turned_q, committed, precision=lax.Precision.HIGHEST)
        * reach_decay[None, :, :, None]
    )
    distance = slot_ids[:, None] - slot_ids[None, :]
    weight = jnp.where(
        distance[None] >= 0.0,
        jnp.exp(log_decay[:, None, None] * jnp.maximum(distance, 0.0)[None]),
        0.0,
    )
    scores = (
        jnp.einsum("sihd,sjhd->shij", turned_q, turned_k, precision=lax.Precision.HIGHEST)
        * weight[None]
    )
    inner_part = jnp.einsum(
        "shij,sjhe->sihe", scores, value_rows.astype(jnp.float32), precision=lax.Precision.HIGHEST
    )
    retained = carried_part + inner_part
    normed = retained * lax.rsqrt(jnp.mean(retained * retained, axis=-1, keepdims=True) + epsilon)
    return (normed.astype(jnp.bfloat16), committed, turned_k)


def body(
    hidden_in,
    norm_gain,
    w_query,
    w_key,
    w_value,
    w_out,
    carried_state,
    prior_keys,
    prior_values,
    accepted,
    lengths,
):
    row_values = hidden_in.astype(jnp.float32)
    normed = (
        row_values
        * lax.rsqrt(jnp.mean(row_values * row_values, axis=-1, keepdims=True) + epsilon)
        * norm_gain
    ).astype(jnp.bfloat16)
    own_rows = normed.shape[0]
    query_width = w_query.shape[1]
    key_width = w_key.shape[1]
    columns = lax.all_to_all(normed, "kv", split_axis=1, concat_axis=0, tiled=True)
    joined = jnp.concatenate((w_query, w_key, w_value), axis=1)
    group_count = lax.axis_size("kv")
    partial_term = jnp.dot(columns, joined, preferred_element_type=jnp.float32)
    grouped = partial_term.reshape(group_count, own_rows, partial_term.shape[1])
    received = lax.all_to_all(grouped, "kv", split_axis=0, concat_axis=0, tiled=True)
    joint_sum = jnp.sum(received, axis=0)
    query_sum = joint_sum[:, :query_width]
    key_sum = joint_sum[:, query_width : query_width + key_width]
    value_sum = joint_sum[:, query_width + key_width :]
    seq_count, head_count, steps_ahead = (
        prior_keys.shape[0],
        prior_keys.shape[1],
        prior_keys.shape[2],
    )

    def by_heads(matrix):
        return matrix.astype(jnp.bfloat16).reshape(seq_count, steps_ahead, head_count, -1)

    value_rows = by_heads(value_sum)
    head_ids = (lax.axis_index("tp") * head_count + jnp.arange(head_count)).astype(jnp.float32)
    heads_out, committed, turned_k = retain(
        by_heads(query_sum),
        by_heads(key_sum),
        value_rows,
        carried_state,
        prior_keys,
        prior_values,
        accepted,
        lengths,
        head_ids,
    )
    flat_rows = heads_out.reshape(own_rows, -1)
    head_terms = lax.dot_general(
        lax.all_gather(flat_rows, "kv", axis=0, tiled=True),
        w_out,
        (((1,), (1,)), ((), ())),
        preferred_element_type=jnp.float32,
    )
    layer_out = lax.psum_scatter(
        head_terms.astype(jnp.bfloat16), "tp", scatter_dimension=0, tiled=True
    )
    new_keys = jnp.transpose(turned_k, (0, 2, 1, 3)).astype(jnp.bfloat16)
    new_values = jnp.transpose(value_rows, (0, 2, 1, 3))
    return (layer_out, committed, new_keys, new_values)


def solution(mesh):
    in_specs = (
        P("kv", None),
        P(),
        P("kv", "tp"),
        P("kv", "tp"),
        P("kv", "tp"),
        P("kv", "tp"),
        P("kv", "tp", None, None),
        P("kv", "tp", None, None),
        P("kv", "tp", None, None),
        P("kv"),
        P("kv"),
    )
    out_specs = (
        P("tp", "kv"),
        P("kv", "tp", None, None),
        P("kv", "tp", None, None),
        P("kv", "tp", None, None),
    )
    return jax.shard_map(body, mesh=mesh, in_specs=in_specs, out_specs=out_specs, check_vma=False)
```

profile of v0, /device:TPU:0, one launch (start us, length us, event | category | flops | bytes accessed | tf_op | source)
XLA Modules:
  0.0 75.1 jit_solution(14520870958238705790)
XLA Ops:
  0.6 1.0 %fusion.6 = f32[3]{0:T(128)S(1)} fusion(bf16[3,4096]{1,0:T(4,128)(2,1)} %param.13), kind=kLoop, calls=%fused_computation.13 | loop fusion | flops 36861 | bytes 24588 | tf_op jit(solution)/shard_map/reduce_sum | solution.py:93
  1.6 1.5 %fusion.8 = bf16[3,4096]{1,0:T(4,128)(2,1)} fusion(bf16[3,4096]{1,0:T(4,128)(2,1)} %param.13, f32[4096]{0:T(1024)} %param.14, f32[3]{0:T(128)S(1)} %add_rsqrt_fusion.1), kind=kLoop, calls=%fused_computation.15 | loop fusion | flops 49152 | bytes 65548 | tf_op jit(solution)/shard_map/convert_element_type | solution.py:95
  3.1 7.3 %all-to-all-start = ((bf16[3,8,512]{2,0,1:T(4,128)(2,1)}), bf16[3,8,512]{2,0,1:T(4,128)(2,1)S(1)}, u32[]{:S(2)}, u32[]{:S(2)}) async-start(bf16[3,8,512]{2,0,1:T(4,128)(2,1)} %bitcast.6), calls=%async_computation | async-start | bytes 65536 | tf_op jit(solution)/shard_map/all_to_all | solution.py:99
  11.9 0.1 fusion.20
  12.0 0.1 multiply_cosine_fusion
  12.2 0.8 %multiply_bitcast_fusion = f32[2,3,256]{2,0,1:T(2,128)S(1)} fusion(bf16[1,2,3,256]{3,1,2,0:T(2,128)(2,1)} %param.20, f32[2,3]{0,1:T(4,128)S(1)} %exponential_select_fusion), kind=kLoop, calls=%fused_computation.28 | loop fusion | flops 3072 | bytes 9240 | tf_op jit(solution)/shard_map/reshape.14
  12.9 1.2 %dynamic-slice.4 = u32[1]{0:T(128)} dynamic-slice(u32[32]{0:T(128)} %constant.49, u32[]{:S(6)} %partition-id.5), dynamic_slice_sizes={1} | dynamic-slice | bytes 12
  14.8 2.2 %all-to-all-done = bf16[3,8,512]{2,0,1:T(4,128)(2,1)S(1)} async-done(((bf16[3,8,512]{2,0,1:T(4,128)(2,1)}), bf16[3,8,512]{2,0,1:T(4,128)(2,1)S(1)}, u32[]{:S(2)}, u32[]{:S(2)}) %all-to-all-start) | async-done | bytes 24608 | tf_op jit(solution)/shard_map/all_to_all | solution.py:99
  17.1 2.0 %fusion.1 = f32[8,3,2048]{2,0,1:T(8,128)S(1)} fusion(bf16[512,1024]{1,0:T(8,128)(2,1)} %param.17, bf16[512,512]{1,0:T(8,128)(2,1)} %param.16, bf16[512,512]{1,0:T(8,128)(2,1)} %param.15, bf16[3,8,512]{2,0,1:T(4,128)(2,1)S(1)} %all-to-all-done), kind=kOutput, calls=%fused_computation.1 | convolution fusion | flops 56623104 | bytes 2318336 | tf_op jit(solution)/shard_map/dot_general | solution.py:102
  19.1 0.8 %copy.24 = f32[8,3,2048]{2,1,0:T(4,128)} copy(f32[8,3,2048]{2,0,1:T(8,128)S(1)} %fusion.1) | data formatting | bytes 393216 | tf_op jit(solution)/shard_map/dot_general | solution.py:102
  19.9 3.8 %all-to-all-start.1 = ((f32[8,3,2048]{2,1,0:T(4,128)}), f32[8,3,2048]{2,1,0:T(4,128)S(1)}, u32[]{:S(2)}, u32[]{:S(2)}) async-start(f32[8,3,2048]{2,1,0:T(4,128)} %copy.24), calls=%async_computation.1 | async-start | bytes 524288 | tf_op jit(solution)/shard_map/all_to_all | solution.py:104
  23.7 0.7 fusion.2
  24.4 7.8 %all-to-all-done.1 = f32[8,3,2048]{2,1,0:T(4,128)S(1)} async-done(((f32[8,3,2048]{2,1,0:T(4,128)}), f32[8,3,2048]{2,1,0:T(4,128)S(1)}, u32[]{:S(2)}, u32[]{:S(2)}) %all-to-all-start.1) | async-done | bytes 196640 | tf_op jit(solution)/shard_map/all_to_all | solution.py:104
  32.3 0.1 convolution_multiply_fusion
  32.4 0.1 convolution_bitcast_fusion.1
  32.6 0.7 multiply_reduce_fusion
  33.3 0.1 multiply_convert_fusion
  33.4 30.5 %all-gather = bf16[8,3,1024]{2,1,0:T(4,128)(2,1)S(1)} all-gather(bf16[1,3,1024]{2,1,0:T(4,128)(2,1)S(1)} %bitcast.60), channel_id=1, replica_groups=mesh['kv'=8,'tp'=4] {'kv'}, dimensions={0}, use_global_device_ids=true | all-gather | bytes 55296 | tf_op jit(solution)/shard_map/all_gather | solution.py:133
  64.0 0.4 convolution_convert_fusion
  64.4 7.5 %fusion = bf16[8,512]{1,0:T(8,128)(2,1)S(1)} fusion(bf16[24,512]{1,0:T(8,128)(2,1)S(1)} %convolution_convert_fusion), kind=kCustom, calls=%all-reduce-scatter | all-reduce-scatter fusion | flops 16385 | bytes 33280
  71.9 1.3 %collective-permute-start = (bf16[6,512]{1,0:T(8,128)(2,1)S(1)}, bf16[6,512]{1,0:T(8,128)(2,1)S(1)}, u32[]{:S(2)}, u32[]{:S(2)}) collective-permute-start(bf16[6,512]{1,0:T(8,128)(2,1)S(1)} %slice.38), channel_id=1, source_target_pairs={{0,1},{1,2},{2,3},{4,5},{5,6},{6,7},{8,9},{9,10},{10,11},{12,13},{... | collective-permute-start | bytes 18440
  73.2 0.6 reshape.407
  73.8 0.6 copy.25
  74.5 0.6 constant_dynamic-slice_fusion
  (32 shorter events, 0.5 us)
Async XLA Ops:
  0.6 63.4 %copy-start = (bf16[512,1024]{1,0:T(8,128)(2,1)S(1)}, bf16[512,1024]{1,0:T(8,128)(2,1)}, u32[]{:S(2)}) copy-start(bf16[512,1024]{1,0:T(8,128)(2,1)} %param.18) | copy-start | bytes 3145732
  3.1 14.0 %all-to-all-start = ((bf16[3,8,512]{2,0,1:T(4,128)(2,1)}), bf16[3,8,512]{2,0,1:T(4,128)(2,1)S(1)}, u32[]{:S(2)}, u32[]{:S(2)}) async-start(bf16[3,8,512]{2,0,1:T(4,128)(2,1)} %bitcast.6), calls=%async_computation | async-start | bytes 65536 | tf_op jit(solution)/shard_map/all_to_all | solution.py:99
  14.8 8.9 %copy-start.3 = (bf16[1,2,3,512]{3,1,2,0:T(2,128)(2,1)S(1)}, bf16[1,2,3,512]{3,1,2,0:T(2,128)(2,1)}, u32[]{:S(2)}) copy-start(bf16[1,2,3,512]{3,1,2,0:T(2,128)(2,1)} %param.21) | copy-start | bytes 18436
  17.1 6.6 %copy-start.2 = (f32[1,2,256,512]{3,2,1,0:T(8,128)S(1)}, f32[1,2,256,512]{3,2,1,0:T(8,128)}, u32[]{:S(2)}) copy-start(f32[1,2,256,512]{3,2,1,0:T(8,128)} %param.19) | copy-start | bytes 3145732
  19.9 12.3 %all-to-all-start.1 = ((f32[8,3,2048]{2,1,0:T(4,128)}), f32[8,3,2048]{2,1,0:T(4,128)S(1)}, u32[]{:S(2)}, u32[]{:S(2)}) async-start(f32[8,3,2048]{2,1,0:T(4,128)} %copy.24), calls=%async_computation.1 | async-start | bytes 524288 | tf_op jit(solution)/shard_map/all_to_all | solution.py:104
  24.4 40.0 %copy-start.1 = (f32[1,2,256,512]{3,2,1,0:T(8,128)}, f32[1,2,256,512]{3,2,1,0:T(8,128)S(1)}, u32[]{:S(2)}) copy-start(f32[1,2,256,512]{3,2,1,0:T(8,128)S(1)} %fusion.2) | copy-start | bytes 3145732
  71.9 2.5 %collective-permute-start = (bf16[6,512]{1,0:T(8,128)(2,1)S(1)}, bf16[6,512]{1,0:T(8,128)(2,1)S(1)}, u32[]{:S(2)}, u32[]{:S(2)}) collective-permute-start(bf16[6,512]{1,0:T(8,128)(2,1)S(1)} %slice.38), channel_id=1, source_target_pairs={{0,1},{1,2},{2,3},{4,5},{5,6},{6,7},{8,9},{9,10},{10,11},{12,13},{... | collective-permute-start | bytes 18440
where the time goes:
time: 76.3 us; the launch traced here: 75.1 us
  blocking collectives  38 us (50%)
  starting transfers between devices  12.3 us (16%)
  waiting for transfers between devices  10 us (13%)
  matrix products  4.06 us (5%)
  local copies, waits for them, and re-layouts  4.05 us (5%)
  other arithmetic  3.82 us (5%)
  between operations  2.77 us (4%)
    all_gather x1, blocking collectives, body(): lax.all_gather(flat_rows, 'kv', axis=0, tiled=True)  30.5 us
    all_to_all x1, waiting for transfers between devices, body(): lax.all_to_all(grouped, 'kv', split_axis=0, concat_axis=0, tiled=True)  7.77 us
    unnamed x1, blocking collectives  7.46 us
    all_to_all x1, starting transfers between devices, body(): lax.all_to_all(normed, 'kv', split_axis=1, concat_axis=0, tiled=True)  7.28 us
    all_to_all x1, starting transfers between devices, body(): lax.all_to_all(grouped, 'kv', split_axis=0, concat_axis=0, tiled=True)  3.77 us
    unnamed x14, local copies, waits for them, and re-layouts  2.59 us
    all_to_all x1, waiting for transfers between devices, body(): lax.all_to_all(normed, 'kv', split_axis=1, concat_axis=0, tiled=True)  2.25 us
    dot_general x1, matrix products, body(): partial_term = jnp.dot(columns, joined, preferred_element_type=jnp.float32)  1.98 us
  transfers between devices with their start and end apart: 3, of which 2 were waited for; matrix products, arithmetic and copies ran while one was open for 6% of the time, Pallas kernels for 0%

commit v1 on v0

--- a/solution.py
+++ b/solution.py
@@ -1,6 +1,11 @@
+import functools
+
 import jax
 import jax.numpy as jnp
+import numpy as np
 from jax import lax
+from jax.experimental import pallas as pl
+from jax.experimental.pallas import tpu as pltpu
 from jax.sharding import PartitionSpec as P
 
 epsilon = 1e-06
@@ -143,6 +148,441 @@
     return (layer_out, committed, new_keys, new_values)
 
 
+MESH_ID = pl.DeviceIdType.MESH
+SUB = 8
+LANE = 128
+
+
+def layer_kernel(
+    kv_size,
+    tp_size,
+    hidden_hbm,
+    gain_hbm,
+    w_query_hbm,
+    w_key_hbm,
+    w_value_hbm,
+    w_out_hbm,
+    carried_hbm,
+    prior_keys_hbm,
+    prior_values_hbm,
+    accepted_hbm,
+    lengths_hbm,
+    inverse_hbm,
+    decay_hbm,
+    layer_out_ref,
+    committed_hbm,
+    new_keys_hbm,
+    new_values_hbm,
+    hidden,
+    gain,
+    w_query,
+    w_key,
+    w_value,
+    w_out,
+    state,
+    state_low,
+    prior_keys,
+    prior_values,
+    accepted,
+    lengths,
+    inverse,
+    decay,
+    normed,
+    own_keys,
+    own_values,
+    rows_recv,
+    rows_pad,
+    part_send_a,
+    part_recv_a,
+    part_send_b,
+    part_recv_b,
+    heads_all,
+    heads_pad,
+    out_send,
+    out_recv,
+    out_rows,
+    load_sems,
+    store_sems,
+    a_send,
+    a_recv,
+    b_send,
+    b_recv,
+    c_send,
+    c_recv,
+    d_send,
+    d_recv,
+):
+    me = lax.axis_index("kv")
+    mine = lax.axis_index("tp")
+    own_rows, width = hidden.shape
+    block = width // kv_size
+    head_count, key_size, value_size = state.shape[1:]
+    half = key_size // 2
+    key_width = head_count * key_size
+    value_width = head_count * value_size
+    per = kv_size // tp_size
+
+    def kv_peer(d):
+        return lax.rem(me + d, kv_size)
+
+    def tp_peer(d):
+        return lax.rem(mine + d, tp_size)
+
+    barrier = pltpu.get_barrier_semaphore()
+    for d in range(1, kv_size):
+        pl.semaphore_signal(barrier, inc=1, device_id={"kv": kv_peer(d)}, device_id_type=MESH_ID)
+    for d in range(1, tp_size):
+        pl.semaphore_signal(barrier, inc=1, device_id={"tp": tp_peer(d)}, device_id_type=MESH_ID)
+
+    pairs = (
+        (hidden_hbm, hidden),
+        (gain_hbm, gain),
+        (accepted_hbm, accepted),
+        (lengths_hbm, lengths),
+        (inverse_hbm, inverse),
+        (decay_hbm, decay),
+        (prior_keys_hbm, prior_keys),
+        (prior_values_hbm, prior_values),
+        (carried_hbm, state),
+        (w_query_hbm, w_query),
+        (w_key_hbm, w_key),
+        (w_value_hbm, w_value),
+        (w_out_hbm, w_out),
+    )
+    loads = [pltpu.make_async_copy(s, t, load_sems.at[k]) for k, (s, t) in enumerate(pairs)]
+    for load in loads:
+        load.start()
+
+    order = sorted(range(1, kv_size), key=lambda d: -min(d, kv_size - d))
+
+    loads[0].wait()
+    loads[1].wait()
+    row_values = hidden[...].astype(jnp.float32)
+    mean = jnp.mean(row_values * row_values, axis=-1, keepdims=True)
+    normed[...] = (row_values * lax.rsqrt(mean + epsilon) * gain[...]).astype(jnp.bfloat16)
+    rows_pad[...] = jnp.zeros_like(rows_pad)
+    heads_pad[...] = jnp.zeros_like(heads_pad)
+
+    pl.semaphore_wait(barrier, kv_size - 1 + tp_size - 1)
+
+    sends = []
+    waits_a = {}
+    for d in order:
+        copy = pltpu.make_async_remote_copy(
+            src_ref=normed.at[:, pl.ds(pl.multiple_of(kv_peer(d) * block, LANE), block)],
+            dst_ref=rows_recv.at[d],
+            send_sem=a_send.at[d],
+            recv_sem=a_recv.at[d],
+            device_id={"kv": kv_peer(d)},
+            device_id_type=MESH_ID,
+        )
+        copy.start()
+        sends.append(copy)
+        waits_a[d] = copy
+
+    for load in loads[2:9]:
+        load.wait()
+    taken = accepted[0]
+    start_place = lengths[0] + taken
+    decays = []
+    for h in range(head_count):
+        g = decay[mine * head_count + h]
+        powers = [jnp.float32(1.0)]
+        for _ in range(own_rows):
+            powers.append(powers[-1] * g)
+        decays.append(powers)
+
+    def power_of(powers, count):
+        out = jnp.float32(0.0)
+        for n, value in enumerate(powers):
+            out = jnp.where(count == n, value, out)
+        return out
+
+    for h in range(head_count):
+        powers = decays[h]
+        keep = power_of(powers, taken)
+        keys = prior_keys[0, h].astype(jnp.float32)
+        values = prior_values[0, h].astype(jnp.float32)
+        padded = jnp.concatenate([keys, jnp.zeros((SUB - own_rows, key_size), jnp.float32)], axis=0)
+        columns = jnp.transpose(padded)
+        total = keep * state[0, h]
+        for j in range(own_rows):
+            weight = power_of(powers, taken - 1 - j)
+            total = total + (columns[:, j : j + 1] * weight) * values[j : j + 1, :]
+        state[0, h] = total
+        state_low[h] = total.astype(jnp.bfloat16)
+    stores = [pltpu.make_async_copy(state, committed_hbm, store_sems.at[0])]
+    stores[0].start()
+
+    step_ids = lax.broadcasted_iota(jnp.int32, (own_rows, half), 0)
+    angles = (step_ids + start_place).astype(jnp.float32) * inverse[...]
+    cosine = jnp.cos(angles)
+    sine = jnp.sin(angles)
+
+    rows_pad[0:own_rows, :] = normed[:, pl.ds(pl.multiple_of(me * block, LANE), block)].astype(jnp.float32)
+    for load in loads[9:12]:
+        load.wait()
+    for d in order:
+        waits_a[d].wait_recv()
+        rows_pad[SUB * d : SUB * d + own_rows, :] = rows_recv[d].astype(jnp.float32)
+    stacked = rows_pad[...].astype(jnp.bfloat16)
+
+    def send_parts(send_ref, recv_ref, chunk):
+        made = []
+        for d in order:
+            e = kv_size - d
+            copy = pltpu.make_async_remote_copy(
+                src_ref=send_ref.at[d],
+                dst_ref=recv_ref.at[e],
+                send_sem=b_send.at[chunk, d],
+                recv_sem=b_recv.at[chunk, e],
+                device_id={"kv": kv_peer(e)},
+                device_id_type=MESH_ID,
+            )
+            copy.start()
+            made.append(copy)
+        return made
+
+    query_part = jnp.dot(stacked, w_query[...], preferred_element_type=jnp.float32)
+    key_part = jnp.dot(stacked, w_key[...], preferred_element_type=jnp.float32)
+    for d in range(kv_size):
+        part_send_a[d, :, 0:key_width] = query_part[SUB * d : SUB * d + own_rows, :].astype(jnp.bfloat16)
+        part_send_a[d, :, key_width:] = key_part[SUB * d : SUB * d + own_rows, :].astype(jnp.bfloat16)
+    made_a = send_parts(part_send_a, part_recv_a, 0)
+    value_part = jnp.dot(stacked, w_value[...], preferred_element_type=jnp.float32)
+    for d in range(kv_size):
+        part_send_b[d] = value_part[SUB * d : SUB * d + own_rows, :].astype(jnp.bfloat16)
+    made_b = send_parts(part_send_b, part_recv_b, 1)
+    sends += made_a + made_b
+
+    joint = jnp.concatenate(
+        [query_part[0:own_rows, :], key_part[0:own_rows, :]], axis=1
+    )
+    for copy in made_a:
+        copy.wait_recv()
+    for d in order:
+        joint = joint + part_recv_a[d].astype(jnp.float32)
+    joint = joint.astype(jnp.bfloat16).astype(jnp.float32)
+
+    def turn(rows):
+        leading = rows[:, :half]
+        trailing = rows[:, half:]
+        return jnp.concatenate(
+            [leading * cosine - trailing * sine, leading * sine + trailing * cosine], axis=1
+        )
+
+    row_ids = lax.broadcasted_iota(jnp.int32, (own_rows, 1), 0)
+    carried_parts = []
+    score_columns = []
+    for h in range(head_count):
+        powers = decays[h]
+        turned_q = turn(joint[:, h * key_size : (h + 1) * key_size])
+        turned_k = turn(joint[:, key_width + h * key_size : key_width + (h + 1) * key_size])
+        turned_k = turned_k * key_size ** (-0.5)
+        own_keys[0, h] = turned_k.astype(jnp.bfloat16)
+        reach = jnp.zeros((own_rows, 1), jnp.float32)
+        for i in range(own_rows):
+            reach = jnp.where(row_ids == i, powers[i + 1], reach)
+        carried_parts.append(
+            jnp.dot(turned_q.astype(jnp.bfloat16), state_low[h], preferred_element_type=jnp.float32)
+            * reach
+        )
+        columns = []
+        for j in range(own_rows):
+            weight = jnp.zeros((own_rows, 1), jnp.float32)
+            for i in range(j, own_rows):
+                weight = jnp.where(row_ids == i, powers[i - j], weight)
+            score = jnp.sum(turned_q * turned_k[j : j + 1, :], axis=-1, keepdims=True)
+            columns.append(score * weight)
+        score_columns.append(columns)
+    stores.append(pltpu.make_async_copy(own_keys, new_keys_hbm, store_sems.at[1]))
+    stores[1].start()
+
+    value_rows = value_part[0:own_rows, :]
+    for copy in made_b:
+        copy.wait_recv()
+    for d in order:
+        value_rows = value_rows + part_recv_b[d].astype(jnp.float32)
+    value_rows = value_rows.astype(jnp.bfloat16).astype(jnp.float32)
+    head_rows = []
+    for h in range(head_count):
+        values = value_rows[:, h * value_size : (h + 1) * value_size]
+        own_values[0, h] = values.astype(jnp.bfloat16)
+        retained = carried_parts[h]
+        for j in range(own_rows):
+            retained = retained + score_columns[h][j] * values[j : j + 1, :]
+        mean = jnp.mean(retained * retained, axis=-1, keepdims=True)
+        head_rows.append(retained * lax.rsqrt(mean + epsilon))
+    heads_all[me] = jnp.concatenate(head_rows, axis=1).astype(jnp.bfloat16)
+
+    waits_c = []
+    for d in order:
+        copy = pltpu.make_async_remote_copy(
+            src_ref=heads_all.at[me],
+            dst_ref=heads_all.at[me],
+            send_sem=c_send.at[d],
+            recv_sem=c_recv.at[d],
+            device_id={"kv": kv_peer(d)},
+            device_id_type=MESH_ID,
+        )
+        copy.start()
+        waits_c.append(copy)
+    sends += waits_c
+    stores.append(pltpu.make_async_copy(own_values, new_values_hbm, store_sems.at[2]))
+    stores[2].start()
+    loads[12].wait()
+    for d in order:
+        pltpu.make_async_remote_copy(
+            src_ref=heads_all.at[me],
+            dst_ref=heads_all.at[kv_peer(kv_size - d)],
+            send_sem=c_send.at[d],
+            recv_sem=c_recv.at[d],
+            device_id={"kv": kv_peer(d)},
+            device_id_type=MESH_ID,
+        ).wait_recv()
+    for j in range(kv_size):
+        heads_pad[SUB * j : SUB * j + own_rows, :] = heads_all[j].astype(jnp.float32)
+    terms = lax.dot_general(
+        heads_pad[...].astype(jnp.bfloat16),
+        w_out[...],
+        (((1,), (1,)), ((), ())),
+        preferred_element_type=jnp.float32,
+    )
+    for t in range(tp_size):
+        for i in range(per):
+            j = t * per + i
+            out_send[t, i] = terms[SUB * j : SUB * j + own_rows, :].astype(jnp.bfloat16)
+    waits_d = []
+    for d in range(1, tp_size):
+        copy = pltpu.make_async_remote_copy(
+            src_ref=out_send.at[tp_peer(d)],
+            dst_ref=out_recv.at[d],
+            send_sem=d_send.at[d],
+            recv_sem=d_recv.at[d],
+            device_id={"tp": tp_peer(d)},
+            device_id_type=MESH_ID,
+        )
+        copy.start()
+        waits_d.append(copy)
+    sends += waits_d
+    own_terms = out_send[mine].astype(jnp.float32)
+    for copy in waits_d:
+        copy.wait_recv()
+    for d in range(1, tp_size):
+        own_terms = own_terms + out_recv[d].astype(jnp.float32)
+    for i in range(per):
+        out_rows[own_rows * i : own_rows * (i + 1), :] = own_terms[i]
+    layer_out_ref[...] = out_rows[...].astype(jnp.bfloat16)
+    for copy in sends:
+        copy.wait_send()
+    for store in stores:
+        store.wait()
+
+
+def fused_body(kv_size, tp_size, *args):
+    hidden_in, norm_gain, w_query, w_key, w_value, w_out, carried_state = args[:7]
+    prior_keys, prior_values, accepted, lengths = args[7:]
+    own_rows, width = hidden_in.shape
+    block = width // kv_size
+    _, head_count, _, key_size = prior_keys.shape
+    value_size = prior_values.shape[-1]
+    half = key_size // 2
+    heads = head_count * tp_size
+    per = kv_size // tp_size
+    inverse = (rotary_base ** (-np.linspace(0.0, 1.0, half))).astype(np.float32)[None, :]
+    decay = (1.0 - 2.0 ** (-5.0 - np.arange(heads))).astype(np.float32)
+    bf16, f32 = jnp.bfloat16, jnp.float32
+    key_width = head_count * key_size
+    value_width = head_count * value_size
+    out_width = w_out.shape[0]
+    any_spec = pl.BlockSpec(memory_space=pl.ANY)
+    return pl.pallas_call(
+        functools.partial(layer_kernel, kv_size, tp_size),
+        out_shape=(
+            jax.ShapeDtypeStruct((per * own_rows, out_width), bf16),
+            jax.ShapeDtypeStruct(carried_state.shape, f32),
+            jax.ShapeDtypeStruct(prior_keys.shape, bf16),
+            jax.ShapeDtypeStruct(prior_values.shape, bf16),
+        ),
+        in_specs=[any_spec] * 13,
+        out_specs=(pl.BlockSpec(memory_space=pltpu.VMEM), any_spec, any_spec, any_spec),
+        scratch_shapes=[
+            pltpu.VMEM(hidden_in.shape, bf16),
+            pltpu.VMEM((1, width), f32),
+            pltpu.VMEM(w_query.shape, bf16),
+            pltpu.VMEM(w_key.shape, bf16),
+            pltpu.VMEM(w_value.shape, bf16),
+            pltpu.VMEM(w_out.shape, bf16),
+            pltpu.VMEM(carried_state.shape, f32),
+            pltpu.VMEM(carried_state.shape[1:], bf16),
+            pltpu.VMEM(prior_keys.shape, bf16),
+            pltpu.VMEM(prior_values.shape, bf16),
+            pltpu.SMEM((1,), jnp.int32),
+            pltpu.SMEM((1,), jnp.int32),
+            pltpu.VMEM((1, half), f32),
+            pltpu.SMEM((heads,), f32),
+            pltpu.VMEM(hidden_in.shape, bf16),
+            pltpu.VMEM(prior_keys.shape, bf16),
+            pltpu.VMEM(prior_values.shape, bf16),
+            pltpu.VMEM((kv_size, own_rows, block), bf16),
+            pltpu.VMEM((kv_size * SUB, block), f32),
+            pltpu.VMEM((kv_size, own_rows, 2 * key_width), bf16),
+            pltpu.VMEM((kv_size, own_rows, 2 * key_width), bf16),
+            pltpu.VMEM((kv_size, own_rows, value_width), bf16),
+            pltpu.VMEM((kv_size, own_rows, value_width), bf16),
+            pltpu.VMEM((kv_size, own_rows, value_width), bf16),
+            pltpu.VMEM((kv_size * SUB, value_width), f32),
+            pltpu.VMEM((tp_size, per, own_rows, out_width), bf16),
+            pltpu.VMEM((tp_size, per, own_rows, out_width), bf16),
+            pltpu.VMEM((per * own_rows, out_width), f32),
+            pltpu.SemaphoreType.DMA((13,)),
+            pltpu.SemaphoreType.DMA((3,)),
+            pltpu.SemaphoreType.DMA((kv_size,)),
+            pltpu.SemaphoreType.DMA((kv_size,)),
+            pltpu.SemaphoreType.DMA((2, kv_size)),
+            pltpu.SemaphoreType.DMA((2, kv_size)),
+            pltpu.SemaphoreType.DMA((kv_size,)),
+            pltpu.SemaphoreType.DMA((kv_size,)),
+            pltpu.SemaphoreType.DMA((tp_size,)),
+            pltpu.SemaphoreType.DMA((tp_size,)),
+        ],
+        compiler_params=pltpu.CompilerParams(collective_id=0, has_side_effects=True),
+    )(
+        hidden_in,
+        norm_gain.reshape(1, width),
+        w_query,
+        w_key,
+        w_value,
+        w_out,
+        carried_state,
+        prior_keys,
+        prior_values,
+        accepted,
+        lengths,
+        inverse,
+        decay,
+    )
+
+
+def kernel_fits(args):
+    hidden_in, w_query, w_out, prior_keys = args[0], args[2], args[5], args[7]
+    kv_size, tp_size = lax.axis_size("kv"), lax.axis_size("tp")
+    return (
+        prior_keys.shape[0] == 1
+        and hidden_in.shape[0] == prior_keys.shape[2] <= SUB
+        and w_query.shape[0] % LANE == 0
+        and w_out.shape[0] % LANE == 0
+        and prior_keys.shape[3] % (2 * LANE) == 0
+        and kv_size % tp_size == 0
+    )
+
+
+def either(*args):
+    if kernel_fits(args):
+        return fused_body(lax.axis_size("kv"), lax.axis_size("tp"), *args)
+    return body(*args)
+
+
 def solution(mesh):
     in_specs = (
         P("kv", None),
@@ -163,4 +603,4 @@
         P("kv", "tp", None, None),
         P("kv", "tp", None, None),
     )
-    return jax.shard_map(body, mesh=mesh, in_specs=in_specs, out_specs=out_specs, check_vma=False)
+    return jax.shard_map(either, mesh=mesh, in_specs=in_specs, out_specs=out_specs, check_vma=False)

time: 76.3 us -> 32.6 us (0.43); the launches traced: 75.1 us -> 32.3 us
  blocking collectives: 38 us -> 0 us
  Pallas kernels: 0 us -> 23.6 us
  starting transfers between devices: 12.3 us -> 0 us
  waiting for transfers between devices: 10 us -> 0 us
  matrix products: 4.06 us -> 0 us
  other arithmetic: 3.82 us -> 0 us
  local copies, waits for them, and re-layouts: 4.05 us -> 6.71 us
  between operations: 2.77 us -> 1.96 us
    all_gather x1 -> x0, blocking collectives: 30.5 us -> none  [body(): lax.all_gather(flat_rows, 'kv', axis=0, tiled=True)]
    pallas_call x0 -> x1, Pallas kernels: none -> 23.6 us  [fused_body(): pl.pallas_call(functools.partial(layer_kernel, kv_size, tp_size), out_sha...]
    all_to_all x2 -> x0, starting transfers between devices: 11.1 us -> none  [the longest x1 7.28 us: body(): lax.all_to_all(normed, 'kv', split_axis=1, concat_axis=0, tiled=True)]
    all_to_all x2 -> x0, waiting for transfers between devices: 10 us -> none  [the longest x1 7.77 us: body(): lax.all_to_all(grouped, 'kv', split_axis=0, concat_axis=0, tiled=True)]
    unnamed x1 -> x0, blocking collectives: 7.46 us -> none
    dot_general x6 -> x0, matrix products: 4.06 us -> none  [the longest x1 1.98 us: body(): partial_term = jnp.dot(columns, joined, preferred_element_type=jnp.float32)]
    unnamed x14 -> x10, local copies, waits for them, and re-layouts: 2.59 us -> 4.85 us
    pallas_call x0 -> x2, local copies, waits for them, and re-layouts: none -> 1.86 us  [fused_body(): pl.pallas_call(functools.partial(layer_kernel, kv_size, tp_size), out_sha...]
  transfers between devices with their start and end apart: 3 -> 0, of which waited for: 2 -> 0; matrix products, arithmetic and copies ran while one was open for 6% -> 0% of each run, Pallas kernels for 0% -> 0%
where the time goes in v1:
time: 32.6 us; the launch traced here: 32.3 us
  Pallas kernels  23.6 us (72%)
  local copies, waits for them, and re-layouts  6.71 us (21%)
  between operations  1.96 us (6%)
    pallas_call x1, Pallas kernels, fused_body(): pl.pallas_call(functools.partial(layer_kernel, kv_size, tp_size), out_sha...  23.6 us
    unnamed x10, local copies, waits for them, and re-layouts  4.85 us
    pallas_call x2, local copies, waits for them, and re-layouts, fused_body(): pl.pallas_call(functools.partial(layer_kernel, kv_size, tp_size), out_sha...  1.86 us

profile of v1, /device:TPU:0, one launch (start us, length us, event | category | flops | bytes accessed | tf_op | source)
XLA Modules:
  0.0 32.3 jit_solution(10656243232584529170)
XLA Ops:
  0.6 0.0 copy-start.2
  1.9 1.3 %copy.17.prior_keys_hbm = bf16[1,2,3,256]{3,2,1,0:T(4,128)(2,1)} copy(bf16[1,2,3,256]{3,1,2,0:T(2,128)(2,1)} %param.20) | data formatting | bytes 6144 | tf_op args[7]
  3.2 0.0 copy-done.2
  3.2 0.6 %copy.18.prior_values_hbm = bf16[1,2,3,512]{3,2,1,0:T(4,128)(2,1)} copy(bf16[1,2,3,512]{3,1,2,0:T(2,128)(2,1)S(1)} %copy-done.2) | data formatting | bytes 12288 | tf_op args[8]
  3.8 23.6 %shard_map.156 = (bf16[6,512]{1,0:T(8,128)(2,1)}, f32[1,2,256,512]{3,2,1,0:T(8,128)}, bf16[1,2,3,256]{3,2,1,0:T(4,128)(2,1)}, bf16[1,2,3,512]{3,2,1,0:T(4,128)(2,1)}) custom-call(bf16[3,4096]{1,0:T(4,128)(2,1)} %hidden_hbm.1, f32[1,4096]{1,0:T(1,128)} %bitcast.1, bf16[512,512]{1,0:T(8,128)(2,1)} %w_query_hbm.1, bf16[512,512]{1,0:T(8,128)(2,1)} %w_key_hbm.1, ...), custom_call_target="tpu_custom_call" | custom-call | tf_op jit(solution)/shard_map/pallas_call | solution.py:499
  27.4 0.0 copy-start
  27.4 1.3 %copy.19 = bf16[1,2,3,256]{3,1,2,0:T(2,128)(2,1)} copy(bf16[1,2,3,256]{3,2,1,0:T(4,128)(2,1)} %get-tuple-element.6) | data formatting | bytes 6144 | tf_op jit(solution)/shard_map/pallas_call | solution.py:499
  28.7 0.0 copy-done
  28.7 0.0 copy-start.1
  28.7 0.6 %copy.20 = bf16[1,2,3,512]{3,1,2,0:T(2,128)(2,1)} copy(bf16[1,2,3,512]{3,2,1,0:T(4,128)(2,1)S(1)} %copy-done) | data formatting | bytes 12288 | tf_op jit(solution)/shard_map/pallas_call | solution.py:499
  29.3 0.1 copy-done.1
  29.4 0.6 %copy.25 = bf16[6,512]{1,0:T(8,128)(2,1)} copy(bf16[6,512]{1,0:T(8,128)(2,1)S(1)} %copy-done.1) | data formatting | bytes 12288
  30.0 2.3 %copy.26 = f32[1,2,256,512]{3,2,1,0:T(8,128)} copy(f32[1,2,256,512]{3,2,1,0:T(8,128)} %get-tuple-element.13) | data formatting | bytes 2097152
Async XLA Ops:
  0.6 2.6 %copy-start.2 = (bf16[1,2,3,512]{3,1,2,0:T(2,128)(2,1)S(1)}, bf16[1,2,3,512]{3,1,2,0:T(2,128)(2,1)}, u32[]{:S(2)}) copy-start(bf16[1,2,3,512]{3,1,2,0:T(2,128)(2,1)} %param.21) | copy-start | bytes 18436
  27.4 1.3 %copy-start = (bf16[1,2,3,512]{3,2,1,0:T(4,128)(2,1)S(1)}, bf16[1,2,3,512]{3,2,1,0:T(4,128)(2,1)}, u32[]{:S(2)}) copy-start(bf16[1,2,3,512]{3,2,1,0:T(4,128)(2,1)} %get-tuple-element.7) | copy-start | bytes 18436
  28.7 0.7 %copy-start.1 = (bf16[6,512]{1,0:T(8,128)(2,1)S(1)}, bf16[6,512]{1,0:T(8,128)(2,1)}, u32[]{:S(2)}) copy-start(bf16[6,512]{1,0:T(8,128)(2,1)} %get-tuple-element.12) | copy-start | bytes 18436

commit v2 on v1

--- a/solution.py
+++ b/solution.py
@@ -170,16 +170,15 @@
     inverse_hbm,
     decay_hbm,
     layer_out_ref,
-    committed_hbm,
-    new_keys_hbm,
-    new_values_hbm,
+    state,
+    own_keys,
+    own_values,
     hidden,
     gain,
     w_query,
     w_key,
     w_value,
     w_out,
-    state,
     state_low,
     prior_keys,
     prior_values,
@@ -188,8 +187,6 @@
     inverse,
     decay,
     normed,
-    own_keys,
-    own_values,
     rows_recv,
     rows_pad,
     part_send_a,
@@ -202,7 +199,6 @@
     out_recv,
     out_rows,
     load_sems,
-    store_sems,
     a_send,
     a_recv,
     b_send,
@@ -301,8 +297,8 @@
     for h in range(head_count):
         powers = decays[h]
         keep = power_of(powers, taken)
-        keys = prior_keys[0, h].astype(jnp.float32)
-        values = prior_values[0, h].astype(jnp.float32)
+        keys = prior_keys[0, :, h, :].astype(jnp.float32)
+        values = prior_values[0, :, h, :].astype(jnp.float32)
         padded = jnp.concatenate([keys, jnp.zeros((SUB - own_rows, key_size), jnp.float32)], axis=0)
         columns = jnp.transpose(padded)
         total = keep * state[0, h]
@@ -311,8 +307,6 @@
             total = total + (columns[:, j : j + 1] * weight) * values[j : j + 1, :]
         state[0, h] = total
         state_low[h] = total.astype(jnp.bfloat16)
-    stores = [pltpu.make_async_copy(state, committed_hbm, store_sems.at[0])]
-    stores[0].start()
 
     step_ids = lax.broadcasted_iota(jnp.int32, (own_rows, half), 0)
     angles = (step_ids + start_place).astype(jnp.float32) * inverse[...]
@@ -379,7 +373,7 @@
         turned_q = turn(joint[:, h * key_size : (h + 1) * key_size])
         turned_k = turn(joint[:, key_width + h * key_size : key_width + (h + 1) * key_size])
         turned_k = turned_k * key_size ** (-0.5)
-        own_keys[0, h] = turned_k.astype(jnp.bfloat16)
+        own_keys[0, :, h, :] = turned_k.astype(jnp.bfloat16)
         reach = jnp.zeros((own_rows, 1), jnp.float32)
         for i in range(own_rows):
             reach = jnp.where(row_ids == i, powers[i + 1], reach)
@@ -395,8 +389,6 @@
             score = jnp.sum(turned_q * turned_k[j : j + 1, :], axis=-1, keepdims=True)
             columns.append(score * weight)
         score_columns.append(columns)
-    stores.append(pltpu.make_async_copy(own_keys, new_keys_hbm, store_sems.at[1]))
-    stores[1].start()
 
     value_rows = value_part[0:own_rows, :]
     for copy in made_b:
@@ -407,7 +399,7 @@
     head_rows = []
     for h in range(head_count):
         values = value_rows[:, h * value_size : (h + 1) * value_size]
-        own_values[0, h] = values.astype(jnp.bfloat16)
+        own_values[0, :, h, :] = values.astype(jnp.bfloat16)
         retained = carried_parts[h]
         for j in range(own_rows):
             retained = retained + score_columns[h][j] * values[j : j + 1, :]
@@ -428,8 +420,6 @@
         copy.start()
         waits_c.append(copy)
     sends += waits_c
-    stores.append(pltpu.make_async_copy(own_values, new_values_hbm, store_sems.at[2]))
-    stores[2].start()
     loads[12].wait()
     for d in order:
         pltpu.make_async_remote_copy(
@@ -475,8 +465,17 @@
     layer_out_ref[...] = out_rows[...].astype(jnp.bfloat16)
     for copy in sends:
         copy.wait_send()
-    for store in stores:
-        store.wait()
+
+
+def finish_kernel(*refs):
+    sources, targets, sems = refs[:4], refs[4:8], refs[8]
+    copies = [
+        pltpu.make_async_copy(s, t, sems.at[k]) for k, (s, t) in enumerate(zip(sources, targets))
+    ]
+    for copy in reversed(copies):
+        copy.start()
+    for copy in copies:
+        copy.wait()
 
 
 def fused_body(kv_size, tp_size, *args):
@@ -485,6 +484,8 @@
     own_rows, width = hidden_in.shape
     block = width // kv_size
     _, head_count, _, key_size = prior_keys.shape
+    prior_keys = jnp.transpose(prior_keys, (0, 2, 1, 3))
+    prior_values = jnp.transpose(prior_values, (0, 2, 1, 3))
     value_size = prior_values.shape[-1]
     half = key_size // 2
     heads = head_count * tp_size
@@ -495,17 +496,18 @@
     key_width = head_count * key_size
     value_width = head_count * value_size
     out_width = w_out.shape[0]
-    any_spec = pl.BlockSpec(memory_space=pl.ANY)
-    return pl.pallas_call(
+    hbm_spec = pl.BlockSpec(memory_space=pltpu.HBM)
+    vmem_spec = pl.BlockSpec(memory_space=pltpu.VMEM)
+    results = pl.pallas_call(
         functools.partial(layer_kernel, kv_size, tp_size),
         out_shape=(
-            jax.ShapeDtypeStruct((per * own_rows, out_width), bf16),
-            jax.ShapeDtypeStruct(carried_state.shape, f32),
-            jax.ShapeDtypeStruct(prior_keys.shape, bf16),
-            jax.ShapeDtypeStruct(prior_values.shape, bf16),
+            pltpu.VMEM((per * own_rows, out_width), bf16),
+            pltpu.VMEM(carried_state.shape, f32),
+            pltpu.VMEM(prior_keys.shape, bf16),
+            pltpu.VMEM(prior_values.shape, bf16),
         ),
-        in_specs=[any_spec] * 13,
-        out_specs=(pl.BlockSpec(memory_space=pltpu.VMEM), any_spec, any_spec, any_spec),
+        in_specs=[hbm_spec] * 13,
+        out_specs=(vmem_spec,) * 4,
         scratch_shapes=[
             pltpu.VMEM(hidden_in.shape, bf16),
             pltpu.VMEM((1, width), f32),
@@ -513,7 +515,6 @@
             pltpu.VMEM(w_key.shape, bf16),
             pltpu.VMEM(w_value.shape, bf16),
             pltpu.VMEM(w_out.shape, bf16),
-            pltpu.VMEM(carried_state.shape, f32),
             pltpu.VMEM(carried_state.shape[1:], bf16),
             pltpu.VMEM(prior_keys.shape, bf16),
             pltpu.VMEM(prior_values.shape, bf16),
@@ -522,8 +523,6 @@
             pltpu.VMEM((1, half), f32),
             pltpu.SMEM((heads,), f32),
             pltpu.VMEM(hidden_in.shape, bf16),
-            pltpu.VMEM(prior_keys.shape, bf16),
-            pltpu.VMEM(prior_values.shape, bf16),
             pltpu.VMEM((kv_size, own_rows, block), bf16),
             pltpu.VMEM((kv_size * SUB, block), f32),
             pltpu.VMEM((kv_size, own_rows, 2 * key_width), bf16),
@@ -536,7 +535,6 @@
             pltpu.VMEM((tp_size, per, own_rows, out_width), bf16),
             pltpu.VMEM((per * own_rows, out_width), f32),
             pltpu.SemaphoreType.DMA((13,)),
-            pltpu.SemaphoreType.DMA((3,)),
             pltpu.SemaphoreType.DMA((kv_size,)),
             pltpu.SemaphoreType.DMA((kv_size,)),
             pltpu.SemaphoreType.DMA((2, kv_size)),
@@ -562,6 +560,19 @@
         inverse,
         decay,
     )
+    layer_out, committed, new_keys, new_values = pl.pallas_call(
+        finish_kernel,
+        out_shape=tuple(jax.ShapeDtypeStruct(r.shape, r.dtype) for r in results),
+        in_specs=[vmem_spec] * 4,
+        out_specs=(hbm_spec,) * 4,
+        scratch_shapes=[pltpu.SemaphoreType.DMA((4,))],
+    )(*[pltpu.with_memory_space_constraint(r, pltpu.VMEM) for r in results])
+    return (
+        layer_out,
+        committed,
+        jnp.transpose(new_keys, (0, 2, 1, 3)),
+        jnp.transpose(new_values, (0, 2, 1, 3)),
+    )
 
 
 def kernel_fits(args):

time: 32.6 us -> 26.2 us (0.80)
  local copies, waits for them, and re-layouts: 6.71 us -> 0 us
  Pallas kernels: 23.6 us -> 24.1 us
    unnamed x10 -> x0, local copies, waits for them, and re-layouts: 4.85 us -> none
    pallas_call x2 -> x0, local copies, waits for them, and re-layouts: 1.86 us -> none  [fused_body(): pl.pallas_call(functools.partial(layer_kernel, kv_size, tp_size), out_sha...]
    pallas_call x0 -> x1, Pallas kernels: none -> 1.02 us  [fused_body(): pl.pallas_call(finish_kernel, out_shape=tuple((jax.ShapeDtypeStruct(r.sha...]
    pallas_call x1, Pallas kernels: 23.6 us -> 23.1 us  [fused_body(): pl.pallas_call(functools.partial(layer_kernel, kv_size, tp_size), out_sha...]
where the time goes in v2:
time: 26.2 us; the launch traced here: 26 us
  Pallas kernels  24.1 us (92%)
  between operations  1.93 us (7%)
    pallas_call x1, Pallas kernels, fused_body(): pl.pallas_call(functools.partial(layer_kernel, kv_size, tp_size), out_sha...  23.1 us
    pallas_call x1, Pallas kernels, fused_body(): pl.pallas_call(finish_kernel, out_shape=tuple((jax.ShapeDtypeStruct(r.sha...  1.02 us

profile of v2, /device:TPU:0, one launch (start us, length us, event | category | flops | bytes accessed | tf_op | source)
XLA Modules:
  0.0 26.0 jit_solution(3021462990671945535)
XLA Ops:
  1.9 23.1 %shard_map.156 = (bf16[6,512]{1,0:T(8,128)(2,1)S(1)}, f32[1,2,256,512]{3,2,1,0:T(8,128)S(1)}, bf16[1,3,2,256]{3,2,1,0:T(2,128)(2,1)S(1)}, bf16[1,3,2,512]{3,2,1,0:T(2,128)(2,1)S(1)}) custom-call(bf16[3,4096]{1,0:T(4,128)(2,1)} %hidden_hbm.1, f32[1,4096]{1,0:T(1,128)} %bitcast.5, bf16[512,512]{1,0:T(8,128)(2,1)} %w_query_hbm.1, bf16[512,512]{1,0:T(8,128)(2,1)} %w_key_hbm.1, ...), custom_call_target="tpu_custom_call" | custom-call | tf_op jit(solution)/shard_map/pallas_call | solution.py:501
  25.0 1.0 %shard_map.157 = (bf16[6,512]{1,0:T(8,128)(2,1)}, f32[1,2,256,512]{3,2,1,0:T(8,128)}, bf16[1,3,2,256]{3,2,1,0:T(2,128)(2,1)}, bf16[1,3,2,512]{3,2,1,0:T(2,128)(2,1)}) custom-call(bf16[6,512]{1,0:T(8,128)(2,1)S(1)} %get-tuple-element.12.refs_0_, f32[1,2,256,512]{3,2,1,0:T(8,128)S(1)} %get-tuple-element.13.refs_1_, ...), custom_call_target="tpu_custom_call" | custom-call | tf_op jit(solution)/shard_map/pallas_call | solution.py:563

commit v3 on v2

--- a/solution.py
+++ b/solution.py
@@ -182,8 +182,6 @@
     state_low,
     prior_keys,
     prior_values,
-    accepted,
-    lengths,
     inverse,
     decay,
     normed,
@@ -193,6 +191,9 @@
     part_recv_a,
     part_send_b,
     part_recv_b,
+    packed,
+    summed_a,
+    summed_b,
     heads_all,
     heads_pad,
     out_send,
@@ -233,8 +234,6 @@
     pairs = (
         (hidden_hbm, hidden),
         (gain_hbm, gain),
-        (accepted_hbm, accepted),
-        (lengths_hbm, lengths),
         (inverse_hbm, inverse),
         (decay_hbm, decay),
         (prior_keys_hbm, prior_keys),
@@ -276,10 +275,10 @@
         sends.append(copy)
         waits_a[d] = copy
 
-    for load in loads[2:9]:
+    for load in loads[2:7]:
         load.wait()
-    taken = accepted[0]
-    start_place = lengths[0] + taken
+    taken = jnp.full((1, 1), accepted_hbm[0], jnp.int32)
+    start_place = lengths_hbm[0] + taken
     decays = []
     for h in range(head_count):
         g = decay[mine * head_count + h]
@@ -289,7 +288,7 @@
         decays.append(powers)
 
     def power_of(powers, count):
-        out = jnp.float32(0.0)
+        out = jnp.zeros(count.shape, jnp.float32)
         for n, value in enumerate(powers):
             out = jnp.where(count == n, value, out)
         return out
@@ -314,12 +313,20 @@
     sine = jnp.sin(angles)
 
     rows_pad[0:own_rows, :] = normed[:, pl.ds(pl.multiple_of(me * block, LANE), block)].astype(jnp.float32)
-    for load in loads[9:12]:
+    for load in loads[7:10]:
         load.wait()
     for d in order:
         waits_a[d].wait_recv()
         rows_pad[SUB * d : SUB * d + own_rows, :] = rows_recv[d].astype(jnp.float32)
     stacked = rows_pad[...].astype(jnp.bfloat16)
+
+    def pack(part, first):
+        for d in range(kv_size):
+            for g in range(part.shape[1] // LANE):
+                low = (first + g) * own_rows
+                packed[d, low : low + own_rows, :] = part[
+                    SUB * d : SUB * d + own_rows, g * LANE : (g + 1) * LANE
+                ]
 
     def send_parts(send_ref, recv_ref, chunk):
         made = []
@@ -339,24 +346,29 @@
 
     query_part = jnp.dot(stacked, w_query[...], preferred_element_type=jnp.float32)
     key_part = jnp.dot(stacked, w_key[...], preferred_element_type=jnp.float32)
-    for d in range(kv_size):
-        part_send_a[d, :, 0:key_width] = query_part[SUB * d : SUB * d + own_rows, :].astype(jnp.bfloat16)
-        part_send_a[d, :, key_width:] = key_part[SUB * d : SUB * d + own_rows, :].astype(jnp.bfloat16)
+    pack(query_part, 0)
+    pack(key_part, key_width // LANE)
+    part_send_a[...] = packed[:, : part_send_a.shape[1], :].astype(jnp.bfloat16)
     made_a = send_parts(part_send_a, part_recv_a, 0)
     value_part = jnp.dot(stacked, w_value[...], preferred_element_type=jnp.float32)
-    for d in range(kv_size):
-        part_send_b[d] = value_part[SUB * d : SUB * d + own_rows, :].astype(jnp.bfloat16)
+    own_a = packed[0, : part_send_a.shape[1], :]
+    pack(value_part, 0)
+    part_send_b[...] = packed[:, : part_send_b.shape[1], :].astype(jnp.bfloat16)
     made_b = send_parts(part_send_b, part_recv_b, 1)
     sends += made_a + made_b
 
-    joint = jnp.concatenate(
-        [query_part[0:own_rows, :], key_part[0:own_rows, :]], axis=1
-    )
+    joint = own_a
     for copy in made_a:
         copy.wait_recv()
     for d in order:
         joint = joint + part_recv_a[d].astype(jnp.float32)
-    joint = joint.astype(jnp.bfloat16).astype(jnp.float32)
+    summed_a[...] = joint.astype(jnp.bfloat16).astype(jnp.float32)
+
+    def unpack(ref, column, size):
+        low = column // LANE
+        return jnp.concatenate(
+            [ref[g * own_rows : (g + 1) * own_rows, :] for g in range(low, low + size // LANE)], axis=1
+        )
 
     def turn(rows):
         leading = rows[:, :half]
@@ -370,8 +382,8 @@
     score_columns = []
     for h in range(head_count):
         powers = decays[h]
-        turned_q = turn(joint[:, h * key_size : (h + 1) * key_size])
-        turned_k = turn(joint[:, key_width + h * key_size : key_width + (h + 1) * key_size])
+        turned_q = turn(unpack(summed_a, h * key_size, key_size))
+        turned_k = turn(unpack(summed_a, key_width + h * key_size, key_size))
         turned_k = turned_k * key_size ** (-0.5)
         own_keys[0, :, h, :] = turned_k.astype(jnp.bfloat16)
         reach = jnp.zeros((own_rows, 1), jnp.float32)
@@ -390,15 +402,15 @@
             columns.append(score * weight)
         score_columns.append(columns)
 
-    value_rows = value_part[0:own_rows, :]
+    value_rows = packed[0, : part_send_b.shape[1], :]
     for copy in made_b:
         copy.wait_recv()
     for d in order:
         value_rows = value_rows + part_recv_b[d].astype(jnp.float32)
-    value_rows = value_rows.astype(jnp.bfloat16).astype(jnp.float32)
+    summed_b[...] = value_rows.astype(jnp.bfloat16).astype(jnp.float32)
     head_rows = []
     for h in range(head_count):
-        values = value_rows[:, h * value_size : (h + 1) * value_size]
+        values = unpack(summed_b, h * value_size, value_size)
         own_values[0, :, h, :] = values.astype(jnp.bfloat16)
         retained = carried_parts[h]
         for j in range(own_rows):
@@ -420,7 +432,7 @@
         copy.start()
         waits_c.append(copy)
     sends += waits_c
-    loads[12].wait()
+    loads[10].wait()
     for d in order:
         pltpu.make_async_remote_copy(
             src_ref=heads_all.at[me],
@@ -496,6 +508,8 @@
     key_width = head_count * key_size
     value_width = head_count * value_size
     out_width = w_out.shape[0]
+    pack_a = own_rows * 2 * key_width // LANE
+    pack_b = own_rows * value_width // LANE
     hbm_spec = pl.BlockSpec(memory_space=pltpu.HBM)
     vmem_spec = pl.BlockSpec(memory_space=pltpu.VMEM)
     results = pl.pallas_call(
@@ -506,7 +520,7 @@
             pltpu.VMEM(prior_keys.shape, bf16),
             pltpu.VMEM(prior_values.shape, bf16),
         ),
-        in_specs=[hbm_spec] * 13,
+        in_specs=[hbm_spec] * 9 + [pl.BlockSpec(memory_space=pltpu.SMEM)] * 2 + [hbm_spec] * 2,
         out_specs=(vmem_spec,) * 4,
         scratch_shapes=[
             pltpu.VMEM(hidden_in.shape, bf16),
@@ -518,23 +532,24 @@
             pltpu.VMEM(carried_state.shape[1:], bf16),
             pltpu.VMEM(prior_keys.shape, bf16),
             pltpu.VMEM(prior_values.shape, bf16),
-            pltpu.SMEM((1,), jnp.int32),
-            pltpu.SMEM((1,), jnp.int32),
             pltpu.VMEM((1, half), f32),
             pltpu.SMEM((heads,), f32),
             pltpu.VMEM(hidden_in.shape, bf16),
             pltpu.VMEM((kv_size, own_rows, block), bf16),
             pltpu.VMEM((kv_size * SUB, block), f32),
-            pltpu.VMEM((kv_size, own_rows, 2 * key_width), bf16),
-            pltpu.VMEM((kv_size, own_rows, 2 * key_width), bf16),
-            pltpu.VMEM((kv_size, own_rows, value_width), bf16),
-            pltpu.VMEM((kv_size, own_rows, value_width), bf16),
+            pltpu.VMEM((kv_size, pack_a, LANE), bf16),
+            pltpu.VMEM((kv_size, pack_a, LANE), bf16),
+            pltpu.VMEM((kv_size, pack_b, LANE), bf16),
+            pltpu.VMEM((kv_size, pack_b, LANE), bf16),
+            pltpu.VMEM((kv_size, max(pack_a, pack_b), LANE), f32),
+            pltpu.VMEM((pack_a, LANE), f32),
+            pltpu.VMEM((pack_b, LANE), f32),
             pltpu.VMEM((kv_size, own_rows, value_width), bf16),
             pltpu.VMEM((kv_size * SUB, value_width), f32),
             pltpu.VMEM((tp_size, per, own_rows, out_width), bf16),
             pltpu.VMEM((tp_size, per, own_rows, out_width), bf16),
             pltpu.VMEM((per * own_rows, out_width), f32),
-            pltpu.SemaphoreType.DMA((13,)),
+            pltpu.SemaphoreType.DMA((11,)),
             pltpu.SemaphoreType.DMA((kv_size,)),
             pltpu.SemaphoreType.DMA((kv_size,)),
             pltpu.SemaphoreType.DMA((2, kv_size)),

time: 26.2 us -> 25.9 us (0.989)
  Pallas kernels: 24.1 us -> 23.8 us
    pallas_call x1, Pallas kernels: 23.1 us -> 22.8 us  [fused_body(): pl.pallas_call(functools.partial(layer_kernel, kv_size, tp_size), out_sha...]
where the time goes in v3:
time: 25.9 us; the launch traced here: 25.8 us
  Pallas kernels  23.8 us (92%)
  between operations  1.93 us (7%)
    pallas_call x1, Pallas kernels, fused_body(): pl.pallas_call(functools.partial(layer_kernel, kv_size, tp_size), out_sha...  22.8 us
    pallas_call x1, Pallas kernels, fused_body(): pl.pallas_call(finish_kernel, out_shape=tuple((jax.ShapeDtypeStruct(r.sha...  1.02 us

profile of v3, /device:TPU:0, one launch (start us, length us, event | category | flops | bytes accessed | tf_op | source)
XLA Modules:
  0.0 25.8 jit_solution(17308162282738392637)
XLA Ops:
  1.9 22.8 %shard_map.156 = (bf16[6,512]{1,0:T(8,128)(2,1)S(1)}, f32[1,2,256,512]{3,2,1,0:T(8,128)S(1)}, bf16[1,3,2,256]{3,2,1,0:T(2,128)(2,1)S(1)}, bf16[1,3,2,512]{3,2,1,0:T(2,128)(2,1)S(1)}) custom-call(bf16[3,4096]{1,0:T(4,128)(2,1)} %hidden_hbm.1, f32[1,4096]{1,0:T(1,128)} %bitcast.5, bf16[512,512]{1,0:T(8,128)(2,1)} %w_query_hbm.1, bf16[512,512]{1,0:T(8,128)(2,1)} %w_key_hbm.1, ...), custom_call_target="tpu_custom_call" | custom-call | tf_op jit(solution)/shard_map/pallas_call | solution.py:515
  24.7 1.0 %shard_map.157 = (bf16[6,512]{1,0:T(8,128)(2,1)}, f32[1,2,256,512]{3,2,1,0:T(8,128)}, bf16[1,3,2,256]{3,2,1,0:T(2,128)(2,1)}, bf16[1,3,2,512]{3,2,1,0:T(2,128)(2,1)}) custom-call(bf16[6,512]{1,0:T(8,128)(2,1)S(1)} %get-tuple-element.12.refs_0_, f32[1,2,256,512]{3,2,1,0:T(8,128)S(1)} %get-tuple-element.13.refs_1_, ...), custom_call_target="tpu_custom_call" | custom-call | tf_op jit(solution)/shard_map/pallas_call | solution.py:578

commit v4 on v3

--- a/solution.py
+++ b/solution.py
@@ -248,7 +248,14 @@
     for load in loads:
         load.start()
 
-    order = sorted(range(1, kv_size), key=lambda d: -min(d, kv_size - d))
+    order = range(1, kv_size)
+
+    def far_offset(k):
+        upper = lax.div(me * 2, kv_size)
+        falling = kv_size - k - lax.div(me + k, kv_size)
+        rising = k - 1 + lax.div(k - 1 - me + kv_size, kv_size)
+        peer = (1 - upper) * falling + upper * rising
+        return lax.rem(peer - me + kv_size, kv_size)
 
     loads[0].wait()
     loads[1].wait()
@@ -261,9 +268,9 @@
     pl.semaphore_wait(barrier, kv_size - 1 + tp_size - 1)
 
     sends = []
-    waits_a = {}
-    for d in order:
-        copy = pltpu.make_async_remote_copy(
+
+    def row_copy(d):
+        return pltpu.make_async_remote_copy(
             src_ref=normed.at[:, pl.ds(pl.multiple_of(kv_peer(d) * block, LANE), block)],
             dst_ref=rows_recv.at[d],
             send_sem=a_send.at[d],
@@ -271,9 +278,11 @@
             device_id={"kv": kv_peer(d)},
             device_id_type=MESH_ID,
         )
-        copy.start()
-        sends.append(copy)
-        waits_a[d] = copy
+
+    for k in order:
+        row_copy(far_offset(k)).start()
+    waits_a = {d: row_copy(d) for d in order}
+    sends += waits_a.values()
 
     for load in loads[2:7]:
         load.wait()
@@ -329,20 +338,19 @@
                 ]
 
     def send_parts(send_ref, recv_ref, chunk):
-        made = []
-        for d in order:
-            e = kv_size - d
-            copy = pltpu.make_async_remote_copy(
-                src_ref=send_ref.at[d],
+        def part_copy(e):
+            return pltpu.make_async_remote_copy(
+                src_ref=send_ref.at[lax.rem(kv_size - e, kv_size)],
                 dst_ref=recv_ref.at[e],
-                send_sem=b_send.at[chunk, d],
+                send_sem=b_send.at[chunk, e],
                 recv_sem=b_recv.at[chunk, e],
                 device_id={"kv": kv_peer(e)},
                 device_id_type=MESH_ID,
             )
-            copy.start()
-            made.append(copy)
-        return made
+
+        for k in order:
+            part_copy(far_offset(k)).start()
+        return [part_copy(e) for e in order]
 
     query_part = jnp.dot(stacked, w_query[...], preferred_element_type=jnp.float32)
     key_part = jnp.dot(stacked, w_key[...], preferred_element_type=jnp.float32)
@@ -419,9 +427,8 @@
         head_rows.append(retained * lax.rsqrt(mean + epsilon))
     heads_all[me] = jnp.concatenate(head_rows, axis=1).astype(jnp.bfloat16)
 
-    waits_c = []
-    for d in order:
-        copy = pltpu.make_async_remote_copy(
+    def head_copy(d):
+        return pltpu.make_async_remote_copy(
             src_ref=heads_all.at[me],
             dst_ref=heads_all.at[me],
             send_sem=c_send.at[d],
@@ -429,9 +436,10 @@
             device_id={"kv": kv_peer(d)},
             device_id_type=MESH_ID,
         )
-        copy.start()
-        waits_c.append(copy)
-    sends += waits_c
+
+    for k in order:
+        head_copy(far_offset(k)).start()
+    sends += [head_copy(d) for d in order]
     loads[10].wait()
     for d in order:
         pltpu.make_async_remote_copy(

time: 25.9 us -> 25.3 us (0.977)
  Pallas kernels: 23.8 us -> 23.2 us
    pallas_call x1, Pallas kernels: 22.8 us -> 22.2 us  [fused_body(): pl.pallas_call(functools.partial(layer_kernel, kv_size, tp_size), out_sha...]
where the time goes in v4:
time: 25.3 us; the launch traced here: 25.1 us
  Pallas kernels  23.2 us (92%)
  between operations  1.93 us (8%)
    pallas_call x1, Pallas kernels, fused_body(): pl.pallas_call(functools.partial(layer_kernel, kv_size, tp_size), out_sha...  22.2 us
    pallas_call x1, Pallas kernels, fused_body(): pl.pallas_call(finish_kernel, out_shape=tuple((jax.ShapeDtypeStruct(r.sha...  1.02 us

profile of v4, /device:TPU:0, one launch (start us, length us, event | category | flops | bytes accessed | tf_op | source)
XLA Modules:
  0.0 25.1 jit_solution(1279449370367278005)
XLA Ops:
  1.9 22.2 %shard_map.156 = (bf16[6,512]{1,0:T(8,128)(2,1)S(1)}, f32[1,2,256,512]{3,2,1,0:T(8,128)S(1)}, bf16[1,3,2,256]{3,2,1,0:T(2,128)(2,1)S(1)}, bf16[1,3,2,512]{3,2,1,0:T(2,128)(2,1)S(1)}) custom-call(bf16[3,4096]{1,0:T(4,128)(2,1)} %hidden_hbm.1, f32[1,4096]{1,0:T(1,128)} %bitcast.5, bf16[512,512]{1,0:T(8,128)(2,1)} %w_query_hbm.1, bf16[512,512]{1,0:T(8,128)(2,1)} %w_key_hbm.1, ...), custom_call_target="tpu_custom_call" | custom-call | tf_op jit(solution)/shard_map/pallas_call | solution.py:523
  24.1 1.0 %shard_map.157 = (bf16[6,512]{1,0:T(8,128)(2,1)}, f32[1,2,256,512]{3,2,1,0:T(8,128)}, bf16[1,3,2,256]{3,2,1,0:T(2,128)(2,1)}, bf16[1,3,2,512]{3,2,1,0:T(2,128)(2,1)}) custom-call(bf16[6,512]{1,0:T(8,128)(2,1)S(1)} %get-tuple-element.12.refs_0_, f32[1,2,256,512]{3,2,1,0:T(8,128)S(1)} %get-tuple-element.13.refs_1_, ...), custom_call_target="tpu_custom_call" | custom-call | tf_op jit(solution)/shard_map/pallas_call | solution.py:586
